TPU v7x, 512 devices: a whole 4x8x8 slice. The times are simulated.
512 devices in a mesh: fs: 128 (over z, y, core), tp: 4 (over x).
Axes of the slice: x: 4, y: 8, z: 8, core: 2. Of those that a mesh axis runs over, the one named last changes fastest.
Arguments:
- inputs: bfloat16 [73728, 2048], P('fs'), may hold values from -24 to 24
- query_cotangent: bfloat16 [73728, 1024], P('fs', 'tp'), may hold values from -0.017944336 to 0.017944336
- value_cotangent: bfloat16 [73728, 1024], P('fs', 'tp'), may hold values from -0.017944336 to 0.017944336
- weights_query: float32 [2048, 1024], P('fs', 'tp'), may hold values from -6 to 6
- weights_value: float32 [2048, 1024], P('fs', 'tp'), may hold values from -6 to 6
- basis_query: bfloat16 [1024, 32], P('tp'), may hold values from -0.75 to 0.75
- basis_value: bfloat16 [1024, 32], P('tp'), may hold values from -0.75 to 0.75
- first_query: float32 [2048, 512], P('fs', 'tp'), may hold values from -5.4 to 5.4, as said below
- second_query: float32 [2048, 512], P('fs', 'tp'), may hold values from 0.05 to 1
- first_value: float32 [2048, 512], P('fs', 'tp'), may hold values from -5.4 to 5.4, as said below
- second_value: float32 [2048, 512], P('fs', 'tp'), may hold values from 0.05 to 1
Outputs:
- step_query: float32 [2048, 1024], P('fs', 'tp')
- step_value: float32 [2048, 1024], P('fs', 'tp')
- new_query: float32 [2048, 1024], P('fs', 'tp')
- new_value: float32 [2048, 1024], P('fs', 'tp')
- copy_query: bfloat16 [2048, 1024], P(None, 'tp')
- copy_value: bfloat16 [2048, 1024], P(None, 'tp')
- moment_query: float32 [2048, 512], P('fs', 'tp')
- square_query: float32 [2048, 512], P('fs', 'tp')
- moment_value: float32 [2048, 512], P('fs', 'tp')
- square_value: float32 [2048, 512], P('fs', 'tp')
Inputs may be any that keep to these rules, and one draw needn't show every extreme that they name: `first_query`: first moments, with a spread of scale from row to row. `first_value`: first moments, with a spread of scale from row to row.
All inputs are finite; a program needn't handle non-finite values.
Results may differ from a plain program's by a relative error of at most 0.003.
Values may be sent and summed in bfloat16 or wider, within the bound.
A program may use at most 64 MiB of HBM per device.

v0:
```python
import jax
import jax.numpy as jnp
from jax import lax
from jax.sharding import Mesh
from jax.sharding import PartitionSpec as P

D = 2048
HEADS = 16
HEAD = 64
RK = 32
FS = ("fs_0", "fs_1", "fs_2")
FS_TP = ("fs_0", "fs_1", "fs_2", "tp")


def reduced_to_own(parts, axes, order):
    dims = [lax.axis_size(a) for a in axes]
    parts = parts.reshape(*dims, *parts.shape[1:])
    parts = parts.transpose(*order, *range(len(axes), parts.ndim))
    parts = parts.reshape(-1, *parts.shape[len(axes) :])
    for k in order:
        parts = lax.psum_scatter(parts, axes[k], scatter_dimension=0, tiled=True)
    return parts[0]


def in_blocks(value, dim, size):
    dims = value.shape
    parts = value.reshape(*dims[:dim], size, dims[dim] // size, *dims[dim + 1 :])
    return jnp.moveaxis(parts, dim, 0)


def scatter_axes(value, axes, order, dim):
    size = lax.axis_size(axes)
    return reduced_to_own(in_blocks(value, dim, size), axes, order)


def one_axis_at_a_time(value, axes):
    for axis in axes:
        value = lax.psum(value, axis)
    return value


def in_one_piece(arrays, axis, dim, along):
    widths = [a.shape[along] for a in arrays]
    both = jnp.concatenate(arrays, axis=along)
    filled = lax.all_gather(both, axis, axis=dim, tiled=True)
    return tuple(jnp.split(filled, [sum(widths[:k]) for k in range(1, len(widths))], axis=along))


def from_space(direction, factor, heads_here):
    count = direction.shape[0]
    split = direction.reshape(count, heads_here, RK)
    out = jnp.einsum("nhr,hdr->nhd", split, factor, precision=lax.Precision.HIGHEST)
    return out.reshape(count, heads_here * HEAD)


def moments(reduced, first, second):
    moment = 0.9 * first + 0.1 * reduced
    square = 0.95 * second + 0.05 * reduced * reduced
    direction = moment / (jnp.sqrt(square) + 1e-08)
    return (moment, square, direction)


def per_device(
    inputs,
    query_cotangent,
    value_cotangent,
    weights_query,
    weights_value,
    basis_query,
    basis_value,
    first_query,
    second_query,
    first_value,
    second_value,
):
    own_cols = weights_query.shape[1]
    heads_here = own_cols // HEAD
    space_cols = heads_here * RK
    factor_q = basis_query.reshape(heads_here, HEAD, RK).astype(jnp.float32)
    factor_v = basis_value.reshape(heads_here, HEAD, RK).astype(jnp.float32)
    contract = (((0,), (0,)), ((), ()))
    tok_count = query_cotangent.shape[0]
    bf_q = basis_query.reshape(heads_here, HEAD, RK)
    bf_v = basis_value.reshape(heads_here, HEAD, RK)
    small_q = jnp.einsum(
        "thd,hdr->thr",
        query_cotangent.reshape(tok_count, heads_here, HEAD),
        bf_q,
        preferred_element_type=jnp.float32,
    )
    small_v = jnp.einsum(
        "thd,hdr->thr",
        value_cotangent.reshape(tok_count, heads_here, HEAD),
        bf_v,
        preferred_element_type=jnp.float32,
    )
    small_both = jnp.concatenate(
        (small_q.reshape(tok_count, space_cols), small_v.reshape(tok_count, space_cols)), axis=1
    )
    upper_part = small_both.astype(jnp.bfloat16)
    lower_part = (small_both - upper_part.astype(jnp.float32)).astype(jnp.bfloat16)
    high = lax.dot_general(inputs, upper_part, contract, preferred_element_type=jnp.float32)
    reduced = scatter_axes(
        high + lax.dot_general(inputs, lower_part, contract, preferred_element_type=jnp.float32),
        FS,
        (2, 0, 1),
        0,
    )
    reduced_q = reduced[:, :space_cols]
    reduced_v = reduced[:, space_cols:]
    moment_q, square_q, direction_q = moments(reduced_q, first_query, second_query)
    moment_v, square_v, direction_v = moments(reduced_v, first_value, second_value)
    total_q, total_v = (
        one_axis_at_a_time(jnp.sum(direction_q * direction_q), FS_TP),
        one_axis_at_a_time(jnp.sum(direction_v * direction_v), FS_TP),
    )
    entries = D * HEADS * RK
    scale_q = 1.0 / jnp.sqrt(total_q / entries + 0.25)
    scale_v = 1.0 / jnp.sqrt(total_v / entries + 0.25)
    step_q = scale_q * from_space(direction_q, factor_q, heads_here)
    step_v = scale_v * from_space(direction_v, factor_v, heads_here)
    fresh_q = weights_query - 0.1 * step_q
    fresh_v = weights_value - 0.1 * step_v
    copy_q, copy_v = in_one_piece(
        (fresh_q.astype(jnp.bfloat16), fresh_v.astype(jnp.bfloat16)), FS, 0, 1
    )
    return (
        step_q,
        step_v,
        fresh_q,
        fresh_v,
        copy_q,
        copy_v,
        moment_q,
        square_q,
        moment_v,
        square_v,
    )


def solution(mesh):
    torus = Mesh(mesh.devices.reshape(8, 8, 2, mesh.shape["tp"]), ("fs_0", "fs_1", "fs_2", "tp"))
    return jax.shard_map(
        per_device,
        mesh=torus,
        in_specs=(
            P(FS, None),
            P(FS, "tp"),
            P(FS, "tp"),
            P(FS, "tp"),
            P(FS, "tp"),
            P("tp", None),
            P("tp", None),
            P(FS, "tp"),
            P(FS, "tp"),
            P(FS, "tp"),
            P(FS, "tp"),
        ),
        out_specs=(
            P(FS, "tp"),
            P(FS, "tp"),
            P(FS, "tp"),
            P(FS, "tp"),
            P(None, "tp"),
            P(None, "tp"),
            P(FS, "tp"),
            P(FS, "tp"),
            P(FS, "tp"),
            P(FS, "tp"),
        ),
        check_vma=False,
    )
```

profile of v0, /device:TPU:1, one launch (start us, length us, event | category | flops | bytes accessed | tf_op | source)
XLA Modules:
  0.0 274.1 jit_solution(18366344088311440782)
XLA Ops:
  7.2 0.0 copy-start
  7.2 0.0 reduce-scatter.4.cloned.1.call-start
  7.2 1.0 reshape.55
  8.2 0.8 reshape.58
  9.0 1.2 copy.41
  10.2 1.2 copy.43
  11.3 0.2 fusion.12
  11.5 0.2 fusion.9
  11.7 0.0 copy-done
  11.7 1.0 fusion.4
  12.7 2.3 fusion
  15.1 2.9 %copy.45 = f32[2048,256]{1,0:T(8,128)} copy(f32[2048,256]{0,1:T(8,128)} %fusion) | data formatting | bytes 4194304 | tf_op jit(solution)/shard_map/add | solution.py:104
  18.0 3.1 %copy.46 = f32[2,8,8,16,256]{4,3,2,1,0:T(8,128)} copy(f32[2,8,8,16,256]{4,3,0,2,1:T(8,128)} %bitcast.28) | data formatting | bytes 4194304 | tf_op jit(solution)/shard_map/transpose | solution.py:18
  21.1 0.0 copy-start.3
  21.1 0.0 copy-start.4
  21.2 0.0 reduce-scatter.4.cloned.1.call-update
  21.2 0.0 reduce-scatter.6.cloned.1.call-start
  21.2 24.5 %reduce-scatter.4.cloned.1.call-done = f32[64,16,256]{2,1,0:T(8,128)} async-done(((f32[128,16,256]{2,1,0:T(8,128)}), f32[64,16,256]{2,1,0:T(8,128)}) %reduce-scatter.4.cloned.1.call-update) | async-done | bytes 1048592 | tf_op jit(solution)/shard_map/reduce_scatter | solution.py:21
  45.7 0.0 reduce-scatter.6.cloned.1.call-update
  45.7 0.0 reduce-scatter.8.cloned.1.call-start
  45.8 41.3 %reduce-scatter.6.cloned.1.call-done = f32[8,16,256]{2,1,0:T(8,128)} async-done(((f32[64,16,256]{2,1,0:T(8,128)}), f32[8,16,256]{2,1,0:T(8,128)}) %reduce-scatter.6.cloned.1.call-update) | async-done | bytes 131088 | tf_op jit(solution)/shard_map/reduce_scatter | solution.py:21
  87.0 0.0 reduce-scatter.8.cloned.1.call-update
  87.0 0.0 all-gather.2.cloned.1.call-start
  87.1 39.1 %reduce-scatter.8.cloned.1.call-done = f32[1,16,256]{2,1,0:T(8,128)} async-done(((f32[8,16,256]{2,1,0:T(8,128)}), f32[1,16,256]{2,1,0:T(8,128)}) %reduce-scatter.8.cloned.1.call-update) | async-done | bytes 16400 | tf_op jit(solution)/shard_map/reduce_scatter | solution.py:21
  126.2 0.0 copy-done.5
  126.2 0.0 copy-done.6
  126.2 0.0 copy-done.7
  126.2 0.0 copy-done.8
  126.2 1.9 multiply_reduce_fusion
  128.1 15.0 %all-reduce.1 = (f32[]{:T(128)}, f32[]{:T(128)}) all-reduce(f32[]{:T(128)} %get-tuple-element.32, f32[]{:T(128)} %get-tuple-element.22), channel_id=1, replica_groups=mesh['fs_0'=8,'fs_1'=8,'fs_2'=2,'tp'=4] {'fs_0'}, use_global_device_ids=true, to_apply=%region_4.0 | all-reduce | flops 2 | bytes 16 | tf_op jit(solution)/shard_map/psum | solution.py:38
  143.1 12.8 %all-reduce = (f32[]{:T(128)}, f32[]{:T(128)}) all-reduce(f32[]{:T(128)} %get-tuple-element.12, f32[]{:T(128)} %get-tuple-element.13), channel_id=1, replica_groups=mesh['fs_0'=8,'fs_1'=8,'fs_2'=2,'tp'=4] {'fs_1'}, use_global_device_ids=true, to_apply=%region_5.0 | all-reduce | flops 2 | bytes 16 | tf_op jit(solution)/shard_map/psum | solution.py:38
  155.9 16.1 %all-reduce.3 = (f32[]{:T(128)}, f32[]{:T(128)}) all-reduce(f32[]{:T(128)} %get-tuple-element.10, f32[]{:T(128)} %get-tuple-element.11), channel_id=1, replica_groups=mesh['fs_0'=8,'fs_1'=8,'fs_2'=2,'tp'=4] {'fs_2'}, use_global_device_ids=true, to_apply=%region_6.0 | all-reduce | flops 2 | bytes 16 | tf_op jit(solution)/shard_map/psum | solution.py:38
  172.0 9.0 %all-reduce.2 = (f32[]{:T(128)}, f32[]{:T(128)}) all-reduce(f32[]{:T(128)} %get-tuple-element.16, f32[]{:T(128)} %get-tuple-element.17), channel_id=1, replica_groups=mesh['fs_0'=8,'fs_1'=8,'fs_2'=2,'tp'=4] {'tp'}, use_global_device_ids=true, to_apply=%region_7.0 | all-reduce | flops 2 | bytes 16 | tf_op jit(solution)/shard_map/psum | solution.py:38
  182.4 0.1 reshape.63
  182.4 0.1 fusion.1
  182.6 0.1 mul.85
  182.7 0.1 reshape.62
  182.8 0.1 fusion.2
  183.0 0.1 mul.75
  183.1 0.0 copy-done.3
  183.1 0.0 copy-done.4
  183.1 0.6 fusion.18
  183.7 0.6 pad_maximum_fusion.1
  184.3 0.0 all-gather.2.cloned.1.call-update
  184.3 80.3 %all-gather.2.cloned.1.call-done = bf16[2048,512]{1,0:T(8,128)(2,1)} async-done(((bf16[16,512]{1,0:T(8,128)(2,1)}), bf16[2048,512]{1,0:T(8,128)(2,1)}) %all-gather.2.cloned.1.call-update) | async-done | bytes 2097168 | tf_op jit(solution)/shard_map/all_gather | solution.py:45
  264.6 3.0 %fusion.22 = (bf16[2048,256]{1,0:T(8,128)(2,1)}, bf16[2048,256]{1,0:T(8,128)(2,1)}) fusion(bf16[2048,512]{1,0:T(8,128)(2,1)} %all-gather.2.cloned.1.call-done), kind=kLoop, calls=%fused_computation.35 | loop fusion | bytes 4194304 | tf_op jit(solution)/shard_map/split | solution.py:46
  267.6 0.0 copy-done.1
  267.6 0.0 copy-done.2
  (8 shorter events, 0.0 us)
Async XLA Ops:
  7.2 4.6 %copy-start = (bf16[576,2048]{1,0:T(8,128)(2,1)S(1)}, bf16[576,2048]{1,0:T(8,128)(2,1)}, u32[]{:S(2)}) copy-start(bf16[576,2048]{1,0:T(8,128)(2,1)} %param.11) | copy-start | bytes 7077892
  7.2 38.5 %reduce-scatter.4.cloned.1.call-start = ((), (), s32[]{:S(2)}) async-start(), calls=%async_computation.3 | async-start | bytes 3145728 | tf_op jit(solution)/shard_map/reduce_scatter | solution.py:21
  21.1 105.0 %copy-start.5 = (f32[16,128]{1,0:T(8,128)S(1)}, f32[16,128]{1,0:T(8,128)}, u32[]{:S(2)}) copy-start(f32[16,128]{1,0:T(8,128)} %param.21) | copy-start | bytes 24580
  21.1 105.0 %copy-start.6 = (f32[16,128]{1,0:T(8,128)S(1)}, f32[16,128]{1,0:T(8,128)}, u32[]{:S(2)}) copy-start(f32[16,128]{1,0:T(8,128)} %param.20) | copy-start | bytes 24580
  21.1 105.0 %copy-start.7 = (f32[16,128]{1,0:T(8,128)S(1)}, f32[16,128]{1,0:T(8,128)}, u32[]{:S(2)}) copy-start(f32[16,128]{1,0:T(8,128)} %param.19) | copy-start | bytes 24580
  21.1 105.0 %copy-start.8 = (f32[16,128]{1,0:T(8,128)S(1)}, f32[16,128]{1,0:T(8,128)}, u32[]{:S(2)}) copy-start(f32[16,128]{1,0:T(8,128)} %param.18) | copy-start | bytes 24580
  21.1 161.9 %copy-start.3 = (f32[16,256]{1,0:T(8,128)S(1)}, f32[16,256]{1,0:T(8,128)}, u32[]{:S(2)}) copy-start(f32[16,256]{1,0:T(8,128)} %param.14) | copy-start | bytes 49156
  21.1 161.9 %copy-start.4 = (f32[16,256]{1,0:T(8,128)S(1)}, f32[16,256]{1,0:T(8,128)}, u32[]{:S(2)}) copy-start(f32[16,256]{1,0:T(8,128)} %param.15) | copy-start | bytes 49156
  21.2 65.8 %reduce-scatter.6.cloned.1.call-start = ((), (), s32[]{:S(2)}) async-start(), calls=%async_computation.4 | async-start | bytes 1179648 | tf_op jit(solution)/shard_map/reduce_scatter | solution.py:21
  45.7 80.5 %reduce-scatter.8.cloned.1.call-start = ((), (), s32[]{:S(2)}) async-start(), calls=%async_computation.5 | async-start | bytes 147456 | tf_op jit(solution)/shard_map/reduce_scatter | solution.py:21
  87.0 177.6 %all-gather.2.cloned.1.call-start = ((), (), s32[]{:S(2)}) async-start(), calls=%async_computation.6 | async-start | bytes 2113536 | tf_op jit(solution)/shard_map/all_gather | solution.py:45
  182.7 84.9 %copy-start.1 = (f32[16,256]{1,0:T(8,128)}, f32[16,256]{1,0:T(8,128)S(1)}, u32[]{:S(2)}) copy-start(f32[16,256]{1,0:T(8,128)S(1)} %mul.85) | copy-start | bytes 49156
  183.1 84.5 %copy-start.2 = (f32[16,256]{1,0:T(8,128)}, f32[16,256]{1,0:T(8,128)S(1)}, u32[]{:S(2)}) copy-start(f32[16,256]{1,0:T(8,128)S(1)} %mul.75) | copy-start | bytes 49156
Sparse Core Ops, SparseCore 0:
  21.3 24.3 reduce-scatter.3
  48.5 38.4 reduce-scatter.5
  89.8 36.3 reduce-scatter.7
  184.4 80.1 all-gather.1
where the time goes:
time: 275 us; the launch traced here: 274 us
  waiting for transfers between devices  185 us (67%)
  blocking collectives  52.9 us (19%)
  between operations  15.3 us (6%)
  local copies, waits for them, and re-layouts  13.6 us (5%)
  matrix products  3.98 us (1%)
  other arithmetic  3.17 us (1%)
    reduce_scatter x3, waiting for transfers between devices, reduced_to_own(): parts = lax.psum_scatter(parts, axes[k], scatter_dimension=0, tiled=True)  105 us
    all_gather x1, waiting for transfers between devices, in_one_piece(): filled = lax.all_gather(both, axis, axis=dim, tiled=True)  80.3 us
    psum x4, blocking collectives, one_axis_at_a_time(): value = lax.psum(value, axis)  52.9 us
  transfers between devices with their start and end apart: 4, of which 4 were waited for; matrix products, arithmetic and copies ran while one was open for 0% of the time, Pallas kernels for 0%

commit v1 on v0

--- a/solution.py
+++ b/solution.py
@@ -35,7 +35,7 @@
 
 def one_axis_at_a_time(value, axes):
     for axis in axes:
-        value = lax.psum(value, axis)
+        value = jnp.sum(lax.all_gather(value, axis), axis=0)
     return value
 
 

time: 275 us -> 292 us (1.062)
  local copies, waits for them, and re-layouts: 13.6 us -> 29.8 us
  other arithmetic: 3.17 us -> 7.98 us
    psum x4 -> x0, blocking collectives: 52.9 us -> none  [one_axis_at_a_time(): value = lax.psum(value, axis)]
    unnamed x0 -> x4, blocking collectives: none -> 50.3 us
    unnamed x20 -> x40, local copies, waits for them, and re-layouts: 2.37 us -> 18.7 us
    reduce_sum x0 -> x8, other arithmetic: none -> 4.81 us  [one_axis_at_a_time(): value = jnp.sum(lax.all_gather(value, axis), axis=0)]
where the time goes in v1:
time: 292 us; the launch traced here: 291 us
  waiting for transfers between devices  184 us (63%)
  blocking collectives  50.3 us (17%)
  local copies, waits for them, and re-layouts  29.8 us (10%)
  between operations  15.3 us (5%)
  other arithmetic  7.98 us (3%)
  matrix products  3.97 us (1%)
    reduce_scatter x3, waiting for transfers between devices, reduced_to_own(): parts = lax.psum_scatter(parts, axes[k], scatter_dimension=0, tiled=True)  104 us
    all_gather x1, waiting for transfers between devices, in_one_piece(): filled = lax.all_gather(both, axis, axis=dim, tiled=True)  80.3 us
    unnamed x4, blocking collectives  50.3 us
    unnamed x40, local copies, waits for them, and re-layouts  18.7 us
  transfers between devices with their start and end apart: 4, of which 4 were waited for; matrix products, arithmetic and copies ran while one was open for 0% of the time, Pallas kernels for 0%

profile of v1, /device:TPU:1, one launch (start us, length us, event | category | flops | bytes accessed | tf_op | source)
XLA Modules:
  0.0 291.4 jit_solution(12437111014980550797)
XLA Ops:
  7.2 1.0 reshape.55
  8.2 0.8 reshape.58
  9.0 1.2 copy.41
  10.2 1.2 copy.43
  11.3 0.2 fusion.12
  11.5 0.2 fusion.9
  11.7 1.0 fusion.4
  12.7 2.3 fusion
  15.0 2.9 %copy.45 = f32[2048,256]{1,0:T(8,128)} copy(f32[2048,256]{0,1:T(8,128)} %fusion) | data formatting | bytes 4194304 | tf_op jit(solution)/shard_map/add | solution.py:104
  18.0 3.1 %copy.46 = f32[2,8,8,16,256]{4,3,2,1,0:T(8,128)} copy(f32[2,8,8,16,256]{4,3,0,2,1:T(8,128)} %bitcast.40) | data formatting | bytes 4194304 | tf_op jit(solution)/shard_map/transpose | solution.py:18
  21.2 24.5 %reduce-scatter.4.cloned.1.call-done = f32[64,16,256]{2,1,0:T(8,128)} async-done(((f32[128,16,256]{2,1,0:T(8,128)}), f32[64,16,256]{2,1,0:T(8,128)}) %reduce-scatter.4.cloned.1.call-update) | async-done | bytes 1048592 | tf_op jit(solution)/shard_map/reduce_scatter | solution.py:21
  45.7 41.3 %reduce-scatter.6.cloned.1.call-done = f32[8,16,256]{2,1,0:T(8,128)} async-done(((f32[64,16,256]{2,1,0:T(8,128)}), f32[8,16,256]{2,1,0:T(8,128)}) %reduce-scatter.6.cloned.1.call-update) | async-done | bytes 131088 | tf_op jit(solution)/shard_map/reduce_scatter | solution.py:21
  87.1 1.3 dynamic-slice
  88.4 37.8 %reduce-scatter.8.cloned.1.call-done = f32[1,16,256]{2,1,0:T(8,128)} async-done(((f32[8,16,256]{2,1,0:T(8,128)}), f32[1,16,256]{2,1,0:T(8,128)}) %reduce-scatter.8.cloned.1.call-update) | async-done | bytes 16400 | tf_op jit(solution)/shard_map/reduce_scatter | solution.py:21
  126.2 1.9 multiply_reduce_fusion
  128.1 1.4 dynamic-update-slice.4
  129.5 1.4 dynamic-update-slice
  130.9 1.3 dynamic-slice.1
  132.2 14.4 %all-reduce.9 = (f32[8]{0:T(128)S(1)}, f32[8]{0:T(128)S(1)}) all-reduce(f32[8]{0:T(128)S(1)} %dynamic-update-slice, f32[8]{0:T(128)S(1)} %dynamic-update-slice.4), channel_id=1, replica_groups=mesh['fs_0'=8,'fs_1'=8,'fs_2'=2,'tp'=4] {'fs_0'}, use_global_device_ids=true, to_apply=%add | all-reduce | flops 16 | bytes 128
  146.5 0.6 reduce_sum.96
  147.1 0.6 reduce_sum.91
  147.7 1.4 dynamic-update-slice.5
  149.1 1.4 dynamic-update-slice.1
  150.5 1.3 dynamic-slice.2
  151.8 11.9 %all-reduce.8 = (f32[8]{0:T(128)S(1)}, f32[8]{0:T(128)S(1)}) all-reduce(f32[8]{0:T(128)S(1)} %dynamic-update-slice.1, f32[8]{0:T(128)S(1)} %dynamic-update-slice.5), channel_id=1, replica_groups=mesh['fs_0'=8,'fs_1'=8,'fs_2'=2,'tp'=4] {'fs_1'}, use_global_device_ids=true, to_apply=%add.1 | all-reduce | flops 16 | bytes 128
  163.7 0.6 reduce_sum.97
  164.3 0.6 reduce_sum.92
  164.9 1.4 dynamic-update-slice.6
  166.3 1.4 dynamic-update-slice.2
  167.7 1.3 dynamic-slice.3
  169.0 15.6 %all-reduce.11 = (f32[2]{0:T(128)S(1)}, f32[2]{0:T(128)S(1)}) all-reduce(f32[2]{0:T(128)S(1)} %dynamic-update-slice.2, f32[2]{0:T(128)S(1)} %dynamic-update-slice.6), channel_id=1, replica_groups=mesh['fs_0'=8,'fs_1'=8,'fs_2'=2,'tp'=4] {'fs_2'}, use_global_device_ids=true, to_apply=%add.2 | all-reduce | flops 4 | bytes 32
  184.7 0.6 reduce_sum.98
  185.3 0.6 reduce_sum.93
  185.9 1.4 dynamic-update-slice.7
  187.3 1.4 dynamic-update-slice.3
  188.7 8.4 %all-reduce.10 = (f32[4]{0:T(128)S(1)}, f32[4]{0:T(128)S(1)}) all-reduce(f32[4]{0:T(128)S(1)} %dynamic-update-slice.3, f32[4]{0:T(128)S(1)} %dynamic-update-slice.7), channel_id=1, replica_groups=mesh['fs_0'=8,'fs_1'=8,'fs_2'=2,'tp'=4] {'tp'}, use_global_device_ids=true, to_apply=%add.3 | all-reduce | flops 8 | bytes 64
  197.1 0.6 reduce_sum.99
  198.4 0.6 reduce_sum.94
  199.7 0.1 reshape.63
  199.7 0.1 fusion.1
  199.9 0.1 mul.85
  200.0 0.1 reshape.62
  200.1 0.1 fusion.2
  200.3 0.1 mul.75
  200.4 0.6 fusion.18
  201.0 0.6 pad_maximum_fusion.1
  201.6 80.3 %all-gather.2.cloned.1.call-done = bf16[2048,512]{1,0:T(8,128)(2,1)} async-done(((bf16[16,512]{1,0:T(8,128)(2,1)}), bf16[2048,512]{1,0:T(8,128)(2,1)}) %all-gather.2.cloned.1.call-update) | async-done | bytes 2097168 | tf_op jit(solution)/shard_map/all_gather | solution.py:45
  281.9 3.0 %fusion.22 = (bf16[2048,256]{1,0:T(8,128)(2,1)}, bf16[2048,256]{1,0:T(8,128)(2,1)}) fusion(bf16[2048,512]{1,0:T(8,128)(2,1)} %all-gather.2.cloned.1.call-done), kind=kLoop, calls=%fused_computation.35 | loop fusion | bytes 4194304 | tf_op jit(solution)/shard_map/split | solution.py:46
  (36 shorter events, 0.3 us)
Async XLA Ops:
  7.2 4.6 %copy-start = (bf16[576,2048]{1,0:T(8,128)(2,1)S(1)}, bf16[576,2048]{1,0:T(8,128)(2,1)}, u32[]{:S(2)}) copy-start(bf16[576,2048]{1,0:T(8,128)(2,1)} %param.11) | copy-start | bytes 7077892
  7.2 38.5 %reduce-scatter.4.cloned.1.call-start = ((), (), s32[]{:S(2)}) async-start(), calls=%async_computation.3 | async-start | bytes 3145728 | tf_op jit(solution)/shard_map/reduce_scatter | solution.py:21
  21.1 105.0 %copy-start.5 = (f32[16,128]{1,0:T(8,128)S(1)}, f32[16,128]{1,0:T(8,128)}, u32[]{:S(2)}) copy-start(f32[16,128]{1,0:T(8,128)} %param.21) | copy-start | bytes 24580
  21.1 105.0 %copy-start.6 = (f32[16,128]{1,0:T(8,128)S(1)}, f32[16,128]{1,0:T(8,128)}, u32[]{:S(2)}) copy-start(f32[16,128]{1,0:T(8,128)} %param.20) | copy-start | bytes 24580
  21.1 105.0 %copy-start.7 = (f32[16,128]{1,0:T(8,128)S(1)}, f32[16,128]{1,0:T(8,128)}, u32[]{:S(2)}) copy-start(f32[16,128]{1,0:T(8,128)} %param.19) | copy-start | bytes 24580
  21.1 105.0 %copy-start.8 = (f32[16,128]{1,0:T(8,128)S(1)}, f32[16,128]{1,0:T(8,128)}, u32[]{:S(2)}) copy-start(f32[16,128]{1,0:T(8,128)} %param.18) | copy-start | bytes 24580
  21.1 179.2 %copy-start.3 = (f32[16,256]{1,0:T(8,128)S(1)}, f32[16,256]{1,0:T(8,128)}, u32[]{:S(2)}) copy-start(f32[16,256]{1,0:T(8,128)} %param.14) | copy-start | bytes 49156
  21.1 179.2 %copy-start.4 = (f32[16,256]{1,0:T(8,128)S(1)}, f32[16,256]{1,0:T(8,128)}, u32[]{:S(2)}) copy-start(f32[16,256]{1,0:T(8,128)} %param.15) | copy-start | bytes 49156
  21.2 65.8 %reduce-scatter.6.cloned.1.call-start = ((), (), s32[]{:S(2)}) async-start(), calls=%async_computation.4 | async-start | bytes 1179648 | tf_op jit(solution)/shard_map/reduce_scatter | solution.py:21
  45.7 80.5 %reduce-scatter.8.cloned.1.call-start = ((), (), s32[]{:S(2)}) async-start(), calls=%async_computation.5 | async-start | bytes 147456 | tf_op jit(solution)/shard_map/reduce_scatter | solution.py:21
  87.0 194.9 %all-gather.2.cloned.1.call-start = ((), (), s32[]{:S(2)}) async-start(), calls=%async_computation.6 | async-start | bytes 2113536 | tf_op jit(solution)/shard_map/all_gather | solution.py:45
  200.0 84.9 %copy-start.1 = (f32[16,256]{1,0:T(8,128)}, f32[16,256]{1,0:T(8,128)S(1)}, u32[]{:S(2)}) copy-start(f32[16,256]{1,0:T(8,128)S(1)} %mul.85) | copy-start | bytes 49156
  200.4 84.5 %copy-start.2 = (f32[16,256]{1,0:T(8,128)}, f32[16,256]{1,0:T(8,128)S(1)}, u32[]{:S(2)}) copy-start(f32[16,256]{1,0:T(8,128)S(1)} %mul.75) | copy-start | bytes 49156
Sparse Core Ops, SparseCore 0:
  21.3 24.3 reduce-scatter.3
  48.5 38.4 reduce-scatter.5
  89.8 36.3 reduce-scatter.7
  201.7 80.1 all-gather.1
